TPU v7x, 32 devices: a whole 2x2x4 slice. The times are simulated.
32 devices in a mesh: fs: 4 (over z), rep: 4 (over y, x), tp: 2 (over core).
Axes of the slice: x: 2, y: 2, z: 4, core: 2. Of those that a mesh axis runs over, the one named last changes fastest.
Arguments:
- saved_inputs: bfloat16 [12288, 2048], P(('fs', 'rep')), may hold values from -6 to 6
- query_cotangent: bfloat16 [12288, 1024], P(('fs', 'rep'), 'tp'), may hold values from -0.053955078 to 0.053955078
- value_cotangent: bfloat16 [12288, 2048], P(('fs', 'rep'), 'tp'), may hold values from -0.053955078 to 0.053955078
- query_weight: float32 [2048, 1024], P('fs', 'tp'), may hold values from -0.125 to 0.125
- value_weight: float32 [2048, 2048], P('fs', 'tp'), may hold values from -0.125 to 0.125
- query_factor: bfloat16 [2048, 256], P('fs'), as said below
- value_factor: bfloat16 [2048, 256], P('fs'), as said below
- query_first: float32 [256, 1024], P('rep', 'tp'), may hold values from -6 to 6
- query_second: float32 [256, 1024], P('rep', 'tp'), may hold values from 0.3 to 3
- value_first: float32 [256, 2048], P('rep', 'tp'), may hold values from -6 to 6
- value_second: float32 [256, 2048], P('rep', 'tp'), may hold values from 0.3 to 3
Outputs:
- query_direction: float32 [2048, 1024], P('fs', 'tp')
- value_direction: float32 [2048, 2048], P('fs', 'tp')
- query_master: float32 [2048, 1024], P('fs', 'tp')
- value_master: float32 [2048, 2048], P('fs', 'tp')
- query_first_new: float32 [256, 1024], P('rep', 'tp')
- query_second_new: float32 [256, 1024], P('rep', 'tp')
- value_first_new: float32 [256, 2048], P('rep', 'tp')
- value_second_new: float32 [256, 2048], P('rep', 'tp')
- query_copy: bfloat16 [2048, 1024], P(None, 'tp')
- value_copy: bfloat16 [2048, 2048], P(None, 'tp')
Inputs may be any that keep to these rules, and one draw needn't show every extreme that they name: `query_factor`: A matrix of full rank. `value_factor`: A matrix of full rank.
All inputs are finite; a program needn't handle non-finite values.
Results may differ from a plain program's by a relative error of at most 0.012.
Values may be sent and summed in bfloat16 or wider, within the bound.
A program may use at most 128 MiB of HBM per device.

v0:
```python
import jax
import jax.numpy as jnp
from jax import lax
from jax.sharding import PartitionSpec as P

BETA_ONE = 0.8
BETA_TWO = 0.9
EPS_RATIO = 1e-08
EPS_NORM = 1e-06
RATE = 0.02


def moments(projected, first, second):
    first_new = BETA_ONE * first + (1.0 - BETA_ONE) * projected
    second_new = BETA_TWO * second + (1.0 - BETA_TWO) * projected * projected
    ratio = first_new / (jnp.sqrt(second_new) + EPS_RATIO)
    return (first_new, second_new, ratio)


def local(
    saved_inputs,
    query_cotangent,
    value_cotangent,
    query_weight,
    value_weight,
    query_factor,
    value_factor,
    query_first,
    query_second,
    value_first,
    value_second,
):
    qc = query_cotangent.shape[1]
    rank = query_factor.shape[1]
    rows = query_weight.shape[0]
    tp = lax.axis_size("tp")
    bf = jnp.bfloat16
    f32 = jnp.float32
    dims = (((0,), (0,)), ((), ()))
    factors = lax.all_gather(
        jnp.concatenate([query_factor, value_factor], axis=1), "fs", axis=0, tiled=True
    )
    weights = lax.all_gather(
        jnp.concatenate([query_weight.astype(bf), value_weight.astype(bf)], axis=1),
        "fs",
        axis=0,
        tiled=True,
    )
    low = jnp.dot(saved_inputs, factors, preferred_element_type=f32).astype(bf)
    proj = jnp.concatenate(
        [
            lax.dot_general(low[:, :rank], query_cotangent, dims, preferred_element_type=f32),
            lax.dot_general(low[:, rank:], value_cotangent, dims, preferred_element_type=f32),
        ],
        axis=1,
    )
    proj = lax.psum_scatter(proj.astype(bf), "rep", scatter_dimension=0, tiled=True)
    proj = lax.psum(proj.astype(f32), "fs")
    query_first_new, query_second_new, query_ratio = moments(
        proj[:, :qc], query_first, query_second
    )
    value_first_new, value_second_new, value_ratio = moments(
        proj[:, qc:], value_first, value_second
    )
    ratio = jnp.concatenate([query_ratio.astype(bf), value_ratio.astype(bf)], axis=1)
    ratio = lax.all_gather(ratio, "rep", axis=0, tiled=True)
    query_raw = jnp.dot(factors[:, :rank], ratio[:, :qc], preferred_element_type=f32)
    value_raw = jnp.dot(factors[:, rank:], ratio[:, qc:], preferred_element_type=f32)
    query_total, value_total = lax.psum(
        (jnp.sum(query_raw * query_raw), jnp.sum(value_raw * value_raw)), "tp"
    )
    query_scale = lax.rsqrt(query_total / (query_raw.size * tp) + EPS_NORM)
    value_scale = lax.rsqrt(value_total / (value_raw.size * tp) + EPS_NORM)
    query_copy = (weights[:, :qc].astype(f32) - RATE * (query_raw * query_scale)).astype(bf)
    value_copy = (weights[:, qc:].astype(f32) - RATE * (value_raw * value_scale)).astype(bf)
    start = lax.axis_index("fs") * rows
    query_direction = lax.dynamic_slice_in_dim(query_raw, start, rows, 0) * query_scale
    value_direction = lax.dynamic_slice_in_dim(value_raw, start, rows, 0) * value_scale
    query_master = query_weight - RATE * query_direction
    value_master = value_weight - RATE * value_direction
    return (
        query_direction,
        value_direction,
        query_master,
        value_master,
        query_first_new,
        query_second_new,
        value_first_new,
        value_second_new,
        query_copy,
        value_copy,
    )


def solution(mesh):
    return jax.shard_map(
        local,
        mesh=mesh,
        in_specs=(
            P(("fs", "rep"), None),
            P(("fs", "rep"), "tp"),
            P(("fs", "rep"), "tp"),
            P("fs", "tp"),
            P("fs", "tp"),
            P("fs", None),
            P("fs", None),
            P("rep", "tp"),
            P("rep", "tp"),
            P("rep", "tp"),
            P("rep", "tp"),
        ),
        out_specs=(
            P("fs", "tp"),
            P("fs", "tp"),
            P("fs", "tp"),
            P("fs", "tp"),
            P("rep", "tp"),
            P("rep", "tp"),
            P("rep", "tp"),
            P("rep", "tp"),
            P(None, "tp"),
            P(None, "tp"),
        ),
        check_vma=False,
    )
```

profile of v0, /device:TPU:0, one launch (start us, length us, event | category | flops | bytes accessed | tf_op | source)
XLA Modules:
  0.0 285.0 jit_solution(16459601803138328107)
XLA Ops:
  7.2 0.0 copy-start
  7.2 0.0 all-gather.3.cloned.1.call-start
  7.2 2.0 pad_maximum_fusion.2
  9.2 0.0 all-gather.3.cloned.1.call-update
  9.3 0.0 reduce-scatter.2.cloned.1.call-start
  9.3 49.2 %all-gather.3.cloned.1.call-done = bf16[2048,512]{1,0:T(8,128)(2,1)} async-done(((bf16[512,512]{1,0:T(8,128)(2,1)}), bf16[2048,512]{1,0:T(8,128)(2,1)}) %all-gather.3.cloned.1.call-update) | async-done | bytes 2097168 | tf_op jit(solution)/shard_map/all_gather | solution.py:40
  58.6 0.0 copy-done
  58.6 0.0 copy-start.4
  58.6 0.0 copy-start.5
  58.6 3.6 %fusion = bf16[768,512]{0,1:T(8,128)(2,1)S(1)} fusion(bf16[2048,512]{1,0:T(8,128)(2,1)} %all-gather.3.cloned.1.call-done, bf16[768,2048]{1,0:T(8,128)(2,1)S(1)} %copy-done), kind=kOutput, calls=%fused_computation.8 | convolution fusion | flops 1611005952 | bytes 6029312 | tf_op jit(solution)/shard_map/dot_general | solution.py:49
  62.1 0.0 copy-done.4
  62.2 0.6 convolution_convert_fusion.1
  62.7 0.0 copy-done.5
  62.8 0.4 convolution_convert_fusion.2
  63.1 0.9 pad_maximum_fusion.1
  64.1 0.0 reduce-scatter.2.cloned.1.call-update
  64.1 0.0 all-gather.5.cloned.1.call-start
  64.1 25.1 %reduce-scatter.2.cloned.1.call-done = bf16[64,1536]{1,0:T(8,128)(2,1)} async-done(((bf16[256,1536]{1,0:T(8,128)(2,1)}), bf16[64,1536]{1,0:T(8,128)(2,1)}) %reduce-scatter.2.cloned.1.call-update) | async-done | bytes 196624 | tf_op jit(solution)/shard_map/reduce_scatter | solution.py:57
  89.2 26.9 %all-reduce.2 = f32[64,1536]{1,0:T(8,128)S(1)} all-reduce(bf16[64,1536]{1,0:T(8,128)(2,1)} %reduce-scatter.2.cloned.1.call-done), channel_id=1, replica_groups=mesh['fs'=4,'rep'=4,'tp'=2] {'fs'}, use_global_device_ids=true, to_apply=%region_1.0 | all-reduce | flops 98304 | bytes 589824 | tf_op jit(solution)/shard_map/psum | solution.py:58
  116.1 0.0 copy-start.2
  116.1 2.1 divide_convert_fusion
  118.2 1.7 divide_convert_fusion.1
  120.0 11.0 %all_gather.10 = bf16[256,1536]{1,0:T(8,128)(2,1)S(1)} all-gather(bf16[64,1536]{1,0:T(8,128)(2,1)S(1)} %pad_maximum_fusion.3), channel_id=1, replica_groups=mesh['fs'=4,'rep'=4,'tp'=2] {'rep'}, dimensions={0}, use_global_device_ids=true | all-gather | bytes 983040 | tf_op jit(solution)/shard_map/all_gather | solution.py:66
  131.0 0.0 copy-done.2
  131.0 3.8 %multiply_reduce_fusion.1 = (f32[]{:T(128)}, f32[2048,512]{1,0:T(8,128)}) fusion(bf16[256,1536]{1,0:T(8,128)(2,1)S(1)} %all_gather.10, bf16[2048,512]{1,0:T(8,128)(2,1)S(1)} %copy-done.2), kind=kOutput, calls=%fused_computation.3 | convolution fusion | flops 538968064 | bytes 5505028 | tf_op jit(solution)/shard_map/dot_general | solution.py:67
  134.8 6.1 %multiply_reduce_fusion = (f32[]{:T(128)}, f32[2048,1024]{1,0:T(8,128)}) fusion(bf16[256,1536]{1,0:T(8,128)(2,1)S(1)} %all_gather.10, bf16[2048,512]{1,0:T(8,128)(2,1)S(1)} %copy-done.2), kind=kOutput, calls=%fused_computation.1 | convolution fusion | flops 1077936128 | bytes 9961476 | tf_op jit(solution)/shard_map/dot_general | solution.py:68
  140.9 3.1 %all-reduce = (f32[]{:T(128)}, f32[]{:T(128)}) all-reduce(f32[]{:T(128)} %get-tuple-element.24, f32[]{:T(128)} %get-tuple-element.26), channel_id=1, replica_groups=mesh['fs'=4,'rep'=4,'tp'=2] {'tp'}, use_global_device_ids=true, to_apply=%region_3.0 | all-reduce | flops 2 | bytes 16 | tf_op jit(solution)/shard_map/psum | solution.py:69
  145.4 0.0 copy-start.3
  145.4 3.6 %multiply_subtract_fusion.1 = (f32[512,512]{1,0:T(8,128)}, f32[512,512]{1,0:T(8,128)}, bf16[512,512]{1,0:T(8,128)(2,1)S(1)}) fusion(f32[512,512]{1,0:T(8,128)} %param.14, f32[]{:T(128)S(6)} %rsqrt.6, f32[2048,512]{1,0:T(8,128)} %get-tuple-element.25, s32[]{:T(128)S(6)} %select_n.4), kind=kLoop, calls=%fused_computation.15 | loop fusion | flops 1048576 | bytes 4718600 | tf_op jit(solution)/shard_map/sub | solution.py:79
  149.0 0.0 copy-done.3
  149.0 4.6 %multiply_subtract_fusion = (f32[512,1024]{1,0:T(8,128)}, f32[512,1024]{1,0:T(8,128)}, bf16[512,1024]{1,0:T(8,128)(2,1)S(1)}) fusion(f32[512,1024]{1,0:T(8,128)S(1)} %copy-done.3, f32[]{:T(128)S(6)} %rsqrt.7, f32[2048,1024]{1,0:T(8,128)} %get-tuple-element.27, s32[]{:T(128)S(6)} %select_n.4), kind=kLoop, calls=%fused_computation.4 | loop fusion | flops 2097152 | bytes 9437192 | tf_op jit(solution)/shard_map/sub | solution.py:80
  153.6 1.2 pad_maximum_fusion
  154.8 0.0 all-gather.5.cloned.1.call-update
  154.9 112.9 %all-gather.5.cloned.1.call-done = bf16[2048,1536]{1,0:T(8,128)(2,1)} async-done(((bf16[512,1536]{1,0:T(8,128)(2,1)}), bf16[2048,1536]{1,0:T(8,128)(2,1)}) %all-gather.5.cloned.1.call-update) | async-done | bytes 6291472 | tf_op jit(solution)/shard_map/all_gather | solution.py:43
  267.7 0.0 copy-start.1
  267.7 5.1 %subtract_convert_fusion.1 = bf16[2048,512]{1,0:T(8,128)(2,1)} fusion(f32[2048,512]{1,0:T(8,128)} %get-tuple-element.25, bf16[2048,1536]{1,0:T(8,128)(2,1)} %all-gather.5.cloned.1.call-done, f32[]{:T(128)S(6)} %rsqrt.6), kind=kLoop, calls=%fused_computation.2 | loop fusion | flops 5242880 | bytes 8388612 | tf_op jit(solution)/shard_map/convert_element_type | solution.py:74
  272.8 0.0 copy-done.1
  272.8 5.7 %subtract_convert_fusion = bf16[2048,1024]{1,0:T(8,128)(2,1)} fusion(f32[2048,1024]{1,0:T(8,128)} %get-tuple-element.27, bf16[2048,1536]{1,0:T(8,128)(2,1)S(1)} %copy-done.1, f32[]{:T(128)S(6)} %rsqrt.7), kind=kLoop, calls=%fused_computation | loop fusion | flops 10485760 | bytes 16777220 | tf_op jit(solution)/shard_map/convert_element_type | solution.py:75
  (1 shorter events, 0.0 us)
Async XLA Ops:
  7.2 51.4 %copy-start = (bf16[768,2048]{1,0:T(8,128)(2,1)S(1)}, bf16[768,2048]{1,0:T(8,128)(2,1)}, u32[]{:S(2)}) copy-start(bf16[768,2048]{1,0:T(8,128)(2,1)} %param.11) | copy-start | bytes 9437188
  7.2 51.4 %all-gather.3.cloned.1.call-start = ((), (), s32[]{:S(2)}) async-start(), calls=%async_computation.1 | async-start | bytes 2621440 | tf_op jit(solution)/shard_map/all_gather | solution.py:40
  9.3 79.9 %reduce-scatter.2.cloned.1.call-start = ((), (), s32[]{:S(2)}) async-start(), calls=%async_computation.2 | async-start | bytes 983040 | tf_op jit(solution)/shard_map/reduce_scatter | solution.py:57
  58.6 3.6 %copy-start.4 = (bf16[768,1024]{1,0:T(8,128)(2,1)S(1)}, bf16[768,1024]{1,0:T(8,128)(2,1)}, u32[]{:S(2)}) copy-start(bf16[768,1024]{1,0:T(8,128)(2,1)} %param.13) | copy-start | bytes 4718596
  58.6 4.2 %copy-start.5 = (bf16[768,512]{1,0:T(8,128)(2,1)S(1)}, bf16[768,512]{1,0:T(8,128)(2,1)}, u32[]{:S(2)}) copy-start(bf16[768,512]{1,0:T(8,128)(2,1)} %param.12) | copy-start | bytes 2359300
  64.1 203.7 %all-gather.5.cloned.1.call-start = ((), (), s32[]{:S(2)}) async-start(), calls=%async_computation.3 | async-start | bytes 7864320 | tf_op jit(solution)/shard_map/all_gather | solution.py:43
  116.1 14.9 %copy-start.2 = (bf16[2048,512]{1,0:T(8,128)(2,1)S(1)}, bf16[2048,512]{1,0:T(8,128)(2,1)}, u32[]{:S(2)}) copy-start(bf16[2048,512]{1,0:T(8,128)(2,1)} %all-gather.3.cloned.1.call-done) | copy-start | bytes 6291460
  145.4 3.7 %copy-start.3 = (f32[512,1024]{1,0:T(8,128)S(1)}, f32[512,1024]{1,0:T(8,128)}, u32[]{:S(2)}) copy-start(f32[512,1024]{1,0:T(8,128)} %param.15) | copy-start | bytes 6291460
  267.7 5.1 %copy-start.1 = (bf16[2048,1536]{1,0:T(8,128)(2,1)S(1)}, bf16[2048,1536]{1,0:T(8,128)(2,1)}, u32[]{:S(2)}) copy-start(bf16[2048,1536]{1,0:T(8,128)(2,1)} %all-gather.5.cloned.1.call-done) | copy-start | bytes 18874372
Sparse Core Ops, SparseCore 0:
  10.1 48.3 all-gather.2
  64.2 24.9 reduce-scatter.1
  155.0 112.7 all-gather.4
where the time goes:
time: 285 us
  waiting for transfers between devices  187 us (66%)
  blocking collectives  41.1 us (14%)
  other arithmetic  27 us (9%)
  between operations  15.2 us (5%)
  matrix products  14.4 us (5%)
    all_gather x1, waiting for transfers between devices, local(): lax.all_gather(jnp.concatenate([query_weight.astype(bf), value_weight.ast...  113 us
    all_gather x1, waiting for transfers between devices, local(): lax.all_gather(jnp.concatenate([query_factor, value_factor], axis=1), 'fs...  49.2 us
    psum x1, blocking collectives, local(): proj = lax.psum(proj.astype(f32), 'fs')  26.9 us
    reduce_scatter x1, waiting for transfers between devices, local(): lax.psum_scatter(proj.astype(bf), 'rep', scatter_dimension=0, tiled=True)  25.1 us
    all_gather x1, blocking collectives, local(): ratio = lax.all_gather(ratio, 'rep', axis=0, tiled=True)  11 us
    dot_general x1, matrix products, local(): jnp.dot(factors[:, rank:], ratio[:, qc:], preferred_element_type=f32)  6.09 us
  transfers between devices with their start and end apart: 3, of which 3 were waited for; matrix products, arithmetic and copies ran while one was open for 0% of the time, Pallas kernels for 0%

commit v1 on v0

--- a/solution.py
+++ b/solution.py
@@ -55,7 +55,9 @@
         axis=1,
     )
     proj = lax.psum_scatter(proj.astype(bf), "rep", scatter_dimension=0, tiled=True)
-    proj = lax.psum(proj.astype(f32), "fs")
+    part = proj.astype(f32)
+    blocks = lax.all_gather(part, "fs", axis=0, tiled=False)
+    proj = blocks.sum(axis=0)
     query_first_new, query_second_new, query_ratio = moments(
         proj[:, :qc], query_first, query_second
     )

time: 285 us -> 300 us (1.053)
  waiting for transfers between devices: 187 us -> 226 us
  blocking collectives: 41.1 us -> 14.1 us
  other arithmetic: 27 us -> 30.2 us
    all_gather x0 -> x1, waiting for transfers between devices: none -> 37.4 us  [local(): blocks = lax.all_gather(part, 'fs', axis=0, tiled=False)]
    psum x1 -> x0, blocking collectives: 26.9 us -> none  [local(): proj = lax.psum(proj.astype(f32), 'fs')]
  transfers between devices with their start and end apart: 3 -> 4, of which waited for: 3 -> 4; matrix products, arithmetic and copies ran while one was open for 0% -> 0% of each run, Pallas kernels for 0% -> 0%
where the time goes in v1:
time: 300 us
  waiting for transfers between devices  226 us (75%)
  other arithmetic  30.2 us (10%)
  between operations  15.2 us (5%)
  matrix products  14.4 us (5%)
  blocking collectives  14.1 us (5%)
    all_gather x1, waiting for transfers between devices, local(): lax.all_gather(jnp.concatenate([query_weight.astype(bf), value_weight.ast...  114 us
    all_gather x1, waiting for transfers between devices, local(): lax.all_gather(jnp.concatenate([query_factor, value_factor], axis=1), 'fs...  49.2 us
    all_gather x1, waiting for transfers between devices, local(): blocks = lax.all_gather(part, 'fs', axis=0, tiled=False)  37.4 us
    reduce_scatter x1, waiting for transfers between devices, local(): lax.psum_scatter(proj.astype(bf), 'rep', scatter_dimension=0, tiled=True)  25.1 us
    all_gather x1, blocking collectives, local(): ratio = lax.all_gather(ratio, 'rep', axis=0, tiled=True)  11.1 us
    dot_general x1, matrix products, local(): jnp.dot(factors[:, rank:], ratio[:, qc:], preferred_element_type=f32)  6.07 us
  transfers between devices with their start and end apart: 4, of which 4 were waited for; matrix products, arithmetic and copies ran while one was open for 0% of the time, Pallas kernels for 0%

profile of v1, /device:TPU:0, one launch (start us, length us, event | category | flops | bytes accessed | tf_op | source)
XLA Modules:
  0.0 299.9 jit_solution(15829503786949996288)
XLA Ops:
  7.2 0.0 copy-start
  7.2 0.0 all-gather.5.cloned.1.call-start
  7.2 2.0 pad_maximum_fusion.2
  9.2 0.0 all-gather.5.cloned.1.call-update
  9.3 0.0 reduce-scatter.2.cloned.1.call-start
  9.3 49.2 %all-gather.5.cloned.1.call-done = bf16[2048,512]{1,0:T(8,128)(2,1)} async-done(((bf16[512,512]{1,0:T(8,128)(2,1)}), bf16[2048,512]{1,0:T(8,128)(2,1)}) %all-gather.5.cloned.1.call-update) | async-done | bytes 2097168 | tf_op jit(solution)/shard_map/all_gather | solution.py:40
  58.6 0.0 copy-done
  58.6 0.0 copy-start.4
  58.6 0.0 copy-start.5
  58.6 3.6 %fusion = bf16[768,512]{0,1:T(8,128)(2,1)S(1)} fusion(bf16[2048,512]{1,0:T(8,128)(2,1)} %all-gather.5.cloned.1.call-done, bf16[768,2048]{1,0:T(8,128)(2,1)S(1)} %copy-done), kind=kOutput, calls=%fused_computation.8 | convolution fusion | flops 1611005952 | bytes 6029312 | tf_op jit(solution)/shard_map/dot_general | solution.py:49
  62.1 0.0 copy-done.4
  62.2 0.6 convolution_convert_fusion.1
  62.7 0.0 copy-done.5
  62.8 0.4 convolution_convert_fusion.2
  63.1 0.9 pad_maximum_fusion.1
  64.1 0.0 reduce-scatter.2.cloned.1.call-update
  64.1 0.0 all-gather.9.cloned.1.call-start
  64.1 25.1 %reduce-scatter.2.cloned.1.call-done = bf16[64,1536]{1,0:T(8,128)(2,1)} async-done(((bf16[256,1536]{1,0:T(8,128)(2,1)}), bf16[64,1536]{1,0:T(8,128)(2,1)}) %reduce-scatter.2.cloned.1.call-update) | async-done | bytes 196624 | tf_op jit(solution)/shard_map/reduce_scatter | solution.py:57
  89.2 1.7 all_gather.24
  90.9 0.0 all-gather.9.cloned.1.call-update
  90.9 0.0 all-gather.7.cloned.1.call-start
  91.0 37.4 %all-gather.9.cloned.1.call-done = f32[256,1536]{1,0:T(8,128)} async-done(((f32[64,1536]{1,0:T(8,128)}), f32[256,1536]{1,0:T(8,128)}) %all-gather.9.cloned.1.call-update) | async-done | bytes 1572880 | tf_op jit(solution)/shard_map/all_gather | solution.py:59
  128.4 1.5 reduce_sum.27
  129.9 0.0 copy-start.2
  129.9 2.1 divide_convert_fusion
  132.0 1.7 divide_convert_fusion.1
  133.8 11.1 %all_gather.22 = bf16[256,1536]{1,0:T(8,128)(2,1)S(1)} all-gather(bf16[64,1536]{1,0:T(8,128)(2,1)S(1)} %pad_maximum_fusion.3), channel_id=1, replica_groups=mesh['fs'=4,'rep'=4,'tp'=2] {'rep'}, dimensions={0}, use_global_device_ids=true | all-gather | bytes 983040 | tf_op jit(solution)/shard_map/all_gather | solution.py:68
  144.8 0.0 copy-done.2
  144.8 3.8 %multiply_reduce_fusion.1 = (f32[]{:T(128)}, f32[2048,512]{1,0:T(8,128)}) fusion(bf16[256,1536]{1,0:T(8,128)(2,1)S(1)} %all_gather.22, bf16[2048,512]{1,0:T(8,128)(2,1)S(1)} %copy-done.2), kind=kOutput, calls=%fused_computation.3 | convolution fusion | flops 538968064 | bytes 5505028 | tf_op jit(solution)/shard_map/dot_general | solution.py:69
  148.6 6.1 %multiply_reduce_fusion = (f32[]{:T(128)}, f32[2048,1024]{1,0:T(8,128)}) fusion(bf16[256,1536]{1,0:T(8,128)(2,1)S(1)} %all_gather.22, bf16[2048,512]{1,0:T(8,128)(2,1)S(1)} %copy-done.2), kind=kOutput, calls=%fused_computation.1 | convolution fusion | flops 1077936128 | bytes 9961476 | tf_op jit(solution)/shard_map/dot_general | solution.py:70
  154.7 3.1 %all-reduce = (f32[]{:T(128)}, f32[]{:T(128)}) all-reduce(f32[]{:T(128)} %get-tuple-element.24, f32[]{:T(128)} %get-tuple-element.26), channel_id=1, replica_groups=mesh['fs'=4,'rep'=4,'tp'=2] {'tp'}, use_global_device_ids=true, to_apply=%region_3.0 | all-reduce | flops 2 | bytes 16 | tf_op jit(solution)/shard_map/psum | solution.py:71
  159.2 0.0 copy-start.3
  159.2 3.6 %multiply_subtract_fusion.1 = (f32[512,512]{1,0:T(8,128)}, f32[512,512]{1,0:T(8,128)}, bf16[512,512]{1,0:T(8,128)(2,1)S(1)}) fusion(f32[512,512]{1,0:T(8,128)} %param.14, f32[]{:T(128)S(6)} %rsqrt.6, f32[2048,512]{1,0:T(8,128)} %get-tuple-element.25, s32[]{:T(128)S(6)} %select_n.4), kind=kLoop, calls=%fused_computation.15 | loop fusion | flops 1048576 | bytes 4718600 | tf_op jit(solution)/shard_map/sub | solution.py:81
  162.8 0.0 copy-done.3
  162.8 4.6 %multiply_subtract_fusion = (f32[512,1024]{1,0:T(8,128)}, f32[512,1024]{1,0:T(8,128)}, bf16[512,1024]{1,0:T(8,128)(2,1)S(1)}) fusion(f32[512,1024]{1,0:T(8,128)S(1)} %copy-done.3, f32[]{:T(128)S(6)} %rsqrt.7, f32[2048,1024]{1,0:T(8,128)} %get-tuple-element.27, s32[]{:T(128)S(6)} %select_n.4), kind=kLoop, calls=%fused_computation.4 | loop fusion | flops 2097152 | bytes 9437192 | tf_op jit(solution)/shard_map/sub | solution.py:82
  167.4 1.2 pad_maximum_fusion
  168.6 0.0 all-gather.7.cloned.1.call-update
  168.7 113.9 %all-gather.7.cloned.1.call-done = bf16[2048,1536]{1,0:T(8,128)(2,1)} async-done(((bf16[512,1536]{1,0:T(8,128)(2,1)}), bf16[2048,1536]{1,0:T(8,128)(2,1)}) %all-gather.7.cloned.1.call-update) | async-done | bytes 6291472 | tf_op jit(solution)/shard_map/all_gather | solution.py:43
  282.6 0.0 copy-start.1
  282.6 5.1 %subtract_convert_fusion.1 = bf16[2048,512]{1,0:T(8,128)(2,1)} fusion(f32[2048,512]{1,0:T(8,128)} %get-tuple-element.25, bf16[2048,1536]{1,0:T(8,128)(2,1)} %all-gather.7.cloned.1.call-done, f32[]{:T(128)S(6)} %rsqrt.6), kind=kLoop, calls=%fused_computation.2 | loop fusion | flops 5242880 | bytes 8388612 | tf_op jit(solution)/shard_map/convert_element_type | solution.py:76
  287.7 0.0 copy-done.1
  287.7 5.7 %subtract_convert_fusion = bf16[2048,1024]{1,0:T(8,128)(2,1)} fusion(f32[2048,1024]{1,0:T(8,128)} %get-tuple-element.27, bf16[2048,1536]{1,0:T(8,128)(2,1)S(1)} %copy-done.1, f32[]{:T(128)S(6)} %rsqrt.7), kind=kLoop, calls=%fused_computation | loop fusion | flops 10485760 | bytes 16777220 | tf_op jit(solution)/shard_map/convert_element_type | solution.py:77
  (1 shorter events, 0.0 us)
Async XLA Ops:
  7.2 51.4 %copy-start = (bf16[768,2048]{1,0:T(8,128)(2,1)S(1)}, bf16[768,2048]{1,0:T(8,128)(2,1)}, u32[]{:S(2)}) copy-start(bf16[768,2048]{1,0:T(8,128)(2,1)} %param.11) | copy-start | bytes 9437188
  7.2 51.4 %all-gather.5.cloned.1.call-start = ((), (), s32[]{:S(2)}) async-start(), calls=%async_computation.1 | async-start | bytes 2621440 | tf_op jit(solution)/shard_map/all_gather | solution.py:40
  9.3 79.9 %reduce-scatter.2.cloned.1.call-start = ((), (), s32[]{:S(2)}) async-start(), calls=%async_computation.2 | async-start | bytes 983040 | tf_op jit(solution)/shard_map/reduce_scatter | solution.py:57
  58.6 3.6 %copy-start.4 = (bf16[768,1024]{1,0:T(8,128)(2,1)S(1)}, bf16[768,1024]{1,0:T(8,128)(2,1)}, u32[]{:S(2)}) copy-start(bf16[768,1024]{1,0:T(8,128)(2,1)} %param.13) | copy-start | bytes 4718596
  58.6 4.2 %copy-start.5 = (bf16[768,512]{1,0:T(8,128)(2,1)S(1)}, bf16[768,512]{1,0:T(8,128)(2,1)}, u32[]{:S(2)}) copy-start(bf16[768,512]{1,0:T(8,128)(2,1)} %param.12) | copy-start | bytes 2359300
  64.1 64.3 %all-gather.9.cloned.1.call-start = ((), (), s32[]{:S(2)}) async-start(), calls=%async_computation.4 | async-start | bytes 1966080 | tf_op jit(solution)/shard_map/all_gather | solution.py:59
  90.9 191.7 %all-gather.7.cloned.1.call-start = ((), (), s32[]{:S(2)}) async-start(), calls=%async_computation.3 | async-start | bytes 7864320 | tf_op jit(solution)/shard_map/all_gather | solution.py:43
  129.9 14.9 %copy-start.2 = (bf16[2048,512]{1,0:T(8,128)(2,1)S(1)}, bf16[2048,512]{1,0:T(8,128)(2,1)}, u32[]{:S(2)}) copy-start(bf16[2048,512]{1,0:T(8,128)(2,1)} %all-gather.5.cloned.1.call-done) | copy-start | bytes 6291460
  159.2 3.7 %copy-start.3 = (f32[512,1024]{1,0:T(8,128)S(1)}, f32[512,1024]{1,0:T(8,128)}, u32[]{:S(2)}) copy-start(f32[512,1024]{1,0:T(8,128)} %param.15) | copy-start | bytes 6291460
  282.6 5.1 %copy-start.1 = (bf16[2048,1536]{1,0:T(8,128)(2,1)S(1)}, bf16[2048,1536]{1,0:T(8,128)(2,1)}, u32[]{:S(2)}) copy-start(bf16[2048,1536]{1,0:T(8,128)(2,1)} %all-gather.7.cloned.1.call-done) | copy-start | bytes 18874372
Sparse Core Ops, SparseCore 0:
  10.1 48.3 all-gather.4
  64.2 24.9 reduce-scatter.1
  91.3 36.9 all-gather.8
  168.8 113.7 all-gather.6
